TPU v7x, 512 devices: a whole 4x8x8 slice. The times are simulated.
512 devices in a mesh: sp: 32 (over z, x), tp: 16 (over y, core).
Axes of the slice: x: 4, y: 8, z: 8, core: 2. Of those that a mesh axis runs over, the one named last changes fastest.
Arguments:
- stream_in: bfloat16 [4096, 2048], P('sp'), may hold values from -8 to 8
- out_cot: bfloat16 [4096, 2048], P('sp'), may hold values from -6 to 6
- route_experts: int32 [4096, 2], P('sp'), may hold values from 0 to 31, all different within a row; in each aligned block of 128 rows (0 to 127, 128 to 255, ...) at most 16 rows name the same one
- route_weights: float32 [4096, 2], P('sp'), may hold values from 0.1 to 1
- w_gate: bfloat16 [32, 2048, 2048], P('sp', None, 'tp'), may hold values from -0.125 to 0.125
- w_up: bfloat16 [32, 2048, 2048], P('sp', None, 'tp'), may hold values from -0.125 to 0.125
- w_down: bfloat16 [32, 2048, 2048], P('sp', 'tp'), may hold values from -0.125 to 0.125
- w_proj: bfloat16 [2048, 1024], P(None, 'tp'), may hold values from -0.1875 to 0.1875
- conv_value: bfloat16 [1024, 4096], P('tp', 'sp'), may hold values from -6 to 6
- conv_gate: bfloat16 [1024, 4096], P('tp', 'sp'), may hold values from -8 to 8
- conv_taps: float32 [31, 1024], P(None, 'tp'), may hold values from -1 to 1
- conv_result: bfloat16 [1024, 4096], P('tp', 'sp'), may hold values from -100 to 100
- channel_norm_gain: float32 [1024], P('tp'), may hold values from 0.1 to 1.9
Outputs:
- grad_gate: bfloat16 [32, 2048, 2048], P('sp', None, 'tp')
- grad_up: bfloat16 [32, 2048, 2048], P('sp', None, 'tp')
- grad_down: bfloat16 [32, 2048, 2048], P('sp', 'tp')
- grad_stream: bfloat16 [4096, 2048], P('sp')
- grad_proj: float32 [2048, 1024], P('sp', 'tp')
- grad_value: bfloat16 [1024, 4096], P('tp', 'sp')
- grad_gate_in: bfloat16 [1024, 4096], P('tp', 'sp')
Inputs may be any that keep to these rules, and one draw needn't show every extreme that they name: `route_experts`: each row names 2 different experts; within each aligned block of 128 rows no expert is named by more than 16 rows, and at least one block reaches that bound for some expert.
All inputs are finite; a program needn't handle non-finite values.
Results may differ from a plain program's by a relative error of at most 0.025.
Values may be sent and summed in bfloat16 or wider, within the bound.
No kernel may reach another device: no remote copies, remote signals or barrier semaphores. Data moves between devices by JAX's collectives and lax.ppermute only.
A program may use at most 64 MiB of HBM per device.

v0:
```python
import jax
import jax.numpy as jnp
from jax import lax
from jax.sharding import PartitionSpec as P

norm_eps = 1e-05
clamp_limit = 7.0
alpha_gate = 1.702


def sent_together(arrays, axis, split_dim, concat_dim, along):
    widths = [a.shape[along] for a in arrays]
    both = jnp.concatenate(arrays, axis=along)
    filled = lax.all_to_all(both, axis, split_axis=split_dim, concat_axis=concat_dim, tiled=True)
    return tuple(jnp.split(filled, [sum(widths[:k]) for k in range(1, len(widths))], axis=along))


def sent_together_2(arrays, axis, dim, along):
    ends, at = ([], 0)
    for a in arrays[:-1]:
        at += a.shape[along]
        ends.append(at)
    both = jnp.concatenate(arrays, axis=along)
    return tuple(jnp.split(lax.all_gather(both, axis, axis=dim, tiled=True), ends, axis=along))


def cut_along(array, dim, devices):
    before, after = (array.shape[:dim], array.shape[dim + 1 :])
    return jnp.moveaxis(array.reshape(*before, devices, -1, *after), dim, 0)


def summed_on_arrival(array, axis, dim):
    tiles = cut_along(array, dim, lax.axis_size(axis))
    arrived = lax.all_to_all(tiles, axis, split_axis=0, concat_axis=0, tiled=True)
    return arrived.astype(jnp.float32).sum(axis=0)


def copy_for_each(array, axis):
    copies = jnp.broadcast_to(array, (lax.axis_size(axis), *array.shape))
    return lax.all_to_all(copies, axis, split_axis=0, concat_axis=0, tiled=True)


def taken_together(array, axis):
    return copy_for_each(array, axis).sum(axis=0)


def packed_total(arrays, axis):
    ends = [0]
    for a in arrays:
        ends.append(ends[-1] + a.size)
    so_far = taken_together(jnp.concatenate([a.ravel() for a in arrays]), axis)
    return tuple((so_far[b:e].reshape(a.shape) for a, b, e in zip(arrays, ends, ends[1:])))


def summed_on_arrival_2(array, axis, dim):
    devices = lax.axis_size(axis)
    tiles = lax.all_to_all(cut_along(array, dim, devices), axis, 0, 0, tiled=True)
    return jnp.sum(tiles, axis=0)


def from_behind(value, axis, steps):
    count = lax.axis_size(axis)
    leading, last = (max(0, -steps), min(count, count - steps))
    return lax.ppermute(value, axis, [(source, source + steps) for source in range(leading, last)])


def slot_tables(block_routes, experts_all, capacity):
    flat_routes = block_routes.reshape(-1)
    assigns = flat_routes.shape[0]
    onehot = (flat_routes[:, None] == jnp.arange(experts_all, dtype=jnp.int32)[None, :]).astype(
        jnp.int32
    )
    before = jnp.cumsum(onehot, axis=0) - onehot
    rank_in = jnp.sum(before * onehot, axis=1)
    slot_of = flat_routes * capacity + rank_in
    source_of = (
        jnp.full((experts_all * capacity,), -1, jnp.int32)
        .at[slot_of]
        .set(jnp.arange(assigns, dtype=jnp.int32))
    )
    return (slot_of, source_of)


def combine_routes(returned, slot_of, cot_cols, token_rows, top_count):
    feature_count = returned.shape[-1]
    flat_back = returned.reshape(-1, feature_count)
    per_route = flat_back[slot_of].astype(jnp.float32).reshape(token_rows, top_count, feature_count)
    return (cot_cols.astype(jnp.float32) + jnp.sum(per_route, axis=1)).astype(jnp.bfloat16)


def expert_terms(rows_in, cot_in, w_gate, w_up, w_down):
    pre_gate = jnp.einsum("secd,edf->secf", rows_in, w_gate, preferred_element_type=jnp.float32)
    pre_up = jnp.einsum("secd,edf->secf", rows_in, w_up, preferred_element_type=jnp.float32)
    glu_part = jnp.minimum(pre_gate, clamp_limit)
    lin_part = jnp.clip(pre_up, -clamp_limit, clamp_limit)
    sig_glu = jax.nn.sigmoid(alpha_gate * glu_part)
    activated = (glu_part * sig_glu * (lin_part + 1.0)).astype(jnp.bfloat16)
    grad_act = jnp.einsum("secd,efd->secf", cot_in, w_down, preferred_element_type=jnp.float32)
    slope = sig_glu + alpha_gate * glu_part * sig_glu * (1.0 - sig_glu)
    grad_pre_gate = jnp.where(
        pre_gate < clamp_limit, grad_act * (lin_part + 1.0) * slope, 0.0
    ).astype(jnp.bfloat16)
    grad_pre_up = jnp.where(
        jnp.abs(pre_up) < clamp_limit, grad_act * glu_part * sig_glu, 0.0
    ).astype(jnp.bfloat16)
    grad_down = jnp.einsum(
        "secf,secd->efd", activated, cot_in, preferred_element_type=jnp.float32
    ).astype(jnp.bfloat16)
    grad_gate = jnp.einsum(
        "secd,secf->edf", rows_in, grad_pre_gate, preferred_element_type=jnp.float32
    ).astype(jnp.bfloat16)
    grad_up = jnp.einsum(
        "secd,secf->edf", rows_in, grad_pre_up, preferred_element_type=jnp.float32
    ).astype(jnp.bfloat16)
    input_part = jnp.einsum(
        "secf,edf->secd", grad_pre_gate, w_gate, preferred_element_type=jnp.float32
    )
    input_part = input_part + jnp.einsum(
        "secf,edf->secd", grad_pre_up, w_up, preferred_element_type=jnp.float32
    )
    return (grad_gate, grad_up, grad_down, input_part)


def body(
    stream_in,
    out_cot,
    route_experts,
    route_weights,
    w_gate,
    w_up,
    w_down,
    w_proj,
    conv_value,
    conv_gate,
    conv_taps,
    conv_result,
    channel_norm_gain,
):
    sp_count = lax.axis_size("sp")
    tp_count = lax.axis_size("tp")
    local_experts = w_gate.shape[0]
    experts_all = local_experts * sp_count
    token_rows, model_width = stream_in.shape
    top_count = route_experts.shape[1]
    capacity = 2 * top_count * token_rows // experts_all
    slot_of, source_of = slot_tables(route_experts, experts_all, capacity)
    occupied = source_of >= 0
    source_safe = jnp.maximum(source_of, 0)
    token_of = source_safe // top_count
    slot_weight = jnp.where(occupied, route_weights.reshape(-1)[source_safe], 0.0)
    row_buffer = jnp.where(occupied[:, None], stream_in[token_of], jnp.zeros((), jnp.bfloat16))
    cot_buffer = (slot_weight[:, None] * out_cot[token_of].astype(jnp.float32)).astype(jnp.bfloat16)
    row_buffer = row_buffer.reshape(experts_all, capacity, model_width)
    cot_buffer = cot_buffer.reshape(experts_all, capacity, model_width)
    slice_width = model_width // tp_count
    slice_start = lax.axis_index("tp") * slice_width
    row_slice = lax.dynamic_slice_in_dim(row_buffer, slice_start, slice_width, 2)
    cot_slice = lax.dynamic_slice_in_dim(cot_buffer, slice_start, slice_width, 2)
    row_slice, cot_slice = sent_together((row_slice, cot_slice), "sp", 0, 0, 1)
    rows_in, cot_in = sent_together_2((row_slice, cot_slice), "tp", 2, 0)
    rows_in = rows_in.reshape(sp_count, local_experts, capacity, model_width)
    cot_in = cot_in.reshape(sp_count, local_experts, capacity, model_width)
    grad_gate, grad_up, grad_down, input_part = expert_terms(rows_in, cot_in, w_gate, w_up, w_down)
    shared = summed_on_arrival(input_part.astype(jnp.bfloat16), "tp", 3)
    returned = shared.astype(jnp.bfloat16).reshape(experts_all, capacity, slice_width)
    returned = lax.all_to_all(returned, "sp", split_axis=0, concat_axis=0, tiled=True)
    cot_cols = lax.dynamic_slice_in_dim(out_cot, slice_start, slice_width, 1)
    stream_part = combine_routes(returned, slot_of, cot_cols, token_rows, top_count)
    grad_stream = lax.all_gather(stream_part, "tp", axis=1, tiled=True)
    channel_total = conv_result.shape[0] * tp_count
    positions = conv_result.shape[1]
    conv_float = conv_result.astype(jnp.float32)
    chan_sum, chan_sq = packed_total(
        (jnp.sum(conv_float, axis=0), jnp.sum(conv_float * conv_float, axis=0)), "tp"
    )
    chan_mean = chan_sum / channel_total
    chan_var = chan_sq / channel_total - chan_mean * chan_mean
    inverse_deviation = lax.rsqrt(chan_var + norm_eps)
    mean_removed = (conv_float - chan_mean) * inverse_deviation
    normalized_rows = mean_removed * channel_norm_gain[:, None]
    sigmoid_of_norm = jax.nn.sigmoid(normalized_rows)
    hidden = (normalized_rows * sigmoid_of_norm).astype(jnp.bfloat16)
    grad_proj = summed_on_arrival_2(
        lax.dot_general(
            grad_stream, hidden, (((0,), (1,)), ((), ())), preferred_element_type=jnp.float32
        ),
        "sp",
        0,
    )
    hidden_gradient = lax.dot_general(
        w_proj, grad_stream, (((0,), (1,)), ((), ())), preferred_element_type=jnp.float32
    )
    normed_input_gradient = (
        hidden_gradient
        * sigmoid_of_norm
        * (1.0 + normalized_rows * (1.0 - sigmoid_of_norm))
        * channel_norm_gain[:, None]
    )
    average_products, cross_products = packed_total(
        (
            jnp.sum(normed_input_gradient, axis=0),
            jnp.sum(normed_input_gradient * mean_removed, axis=0),
        ),
        "tp",
    )
    conv_output_gradient = inverse_deviation * (
        normed_input_gradient
        - average_products / channel_total
        - mean_removed * (cross_products / channel_total)
    )
    taps_count = conv_taps.shape[0]
    next_rim = from_behind(conv_output_gradient[:, : taps_count - 1], "sp", -1)
    extended = jnp.concatenate([conv_output_gradient, next_rim], axis=1)
    grad_gated = jnp.zeros_like(conv_output_gradient)
    for tap_index in range(taps_count):
        grad_gated = (
            grad_gated
            + conv_taps[tap_index][:, None] * extended[:, tap_index : tap_index + positions]
        )
    gate_sig = jax.nn.sigmoid(conv_gate.astype(jnp.float32))
    grad_value = (grad_gated * gate_sig).astype(jnp.bfloat16)
    grad_gate_in = (
        grad_gated * conv_value.astype(jnp.float32) * gate_sig * (1.0 - gate_sig)
    ).astype(jnp.bfloat16)
    return (grad_gate, grad_up, grad_down, grad_stream, grad_proj, grad_value, grad_gate_in)


def solution(mesh):
    return jax.shard_map(
        body,
        mesh=mesh,
        in_specs=(
            P("sp", None),
            P("sp", None),
            P("sp", None),
            P("sp", None),
            P("sp", None, "tp"),
            P("sp", None, "tp"),
            P("sp", "tp", None),
            P(None, "tp"),
            P("tp", "sp"),
            P("tp", "sp"),
            P(None, "tp"),
            P("tp", "sp"),
            P("tp"),
        ),
        out_specs=(
            P("sp", None, "tp"),
            P("sp", None, "tp"),
            P("sp", "tp", None),
            P("sp", None),
            P("sp", "tp"),
            P("tp", "sp"),
            P("tp", "sp"),
        ),
        check_vma=False,
    )
```

profile of v0, /device:TPU:1, one launch (start us, length us, event | category | flops | bytes accessed | tf_op | source)
XLA Modules:
  0.0 249.6 jit_solution(8566486393356843198)
XLA Ops:
  12.7 3.5 %gather_fusion.1 = f32[512]{0:T(512)S(1)} fusion(f32[256]{0:T(256)S(1)} %reshape.203, s32[1024]{0:T(1024)S(1)} %get-tuple-element.78), kind=kCustom, calls=%fused_computation.1 | custom fusion | bytes 6144 | tf_op jit(solution)/shard_map/gather | solution.py:150
  16.3 3.3 %gather_fusion.2 = bf16[512,2048]{1,0:T(8,128)(2,1)} fusion(bf16[128,2048]{1,0:T(8,128)(2,1)S(1)} %copy-done.1, s32[1024]{0:T(1024)S(1)} %get-tuple-element.79), kind=kCustom, calls=%fused_computation.2 | custom fusion | bytes 4196352 | tf_op jit(solution)/shard_map/gather | solution.py:152
  19.6 3.3 %gather_fusion = bf16[512,2048]{1,0:T(8,128)(2,1)} fusion(bf16[128,2048]{1,0:T(8,128)(2,1)S(1)} %copy-done.2, s32[1024]{0:T(1024)S(1)} %get-tuple-element.79), kind=kCustom, calls=%fused_computation | custom fusion | bytes 4196352 | tf_op jit(solution)/shard_map/gather | solution.py:151
  25.1 24.9 %all_to_all.32 = bf16[32,32,128]{2,1,0:T(8,128)(2,1)S(1)} all-to-all(bf16[32,32,128]{2,1,0:T(8,128)(2,1)S(1)} %pad_maximum_fusion), channel_id=1, replica_groups=mesh['sp'=32,'tp'=16] {'sp'}, dimensions={0} | all-to-all | bytes 524288 | tf_op jit(solution)/shard_map/all_to_all | solution.py:14
  51.5 9.6 %all-to-all-start.3 = ((f32[16,1,256]{2,1,0:T(1,128)}), f32[16,1,256]{2,1,0:T(1,128)S(1)}, u32[]{:S(2)}, u32[]{:S(2)}) async-start(f32[16,1,256]{2,1,0:T(1,128)} %broadcast_in_dim.59), calls=%async_computation.3 | async-start | bytes 32768 | tf_op jit(solution)/shard_map/all_to_all | solution.py:40
  61.1 39.7 %all-gather.2.cloned.1.call-done = bf16[64,16,2048]{2,1,0:T(8,128)(2,1)} async-done(((bf16[64,16,128]{2,1,0:T(8,128)(2,1)}), bf16[64,16,2048]{2,1,0:T(8,128)(2,1)}) %all-gather.2.cloned.1.call-update) | async-done | bytes 4194320 | tf_op jit(solution)/shard_map/all_gather | solution.py:24
  100.8 2.4 fusion.12
  103.2 2.3 fusion.17
  107.8 1.9 copy.78
  110.4 4.7 %all-to-all-start.1 = ((bf16[16,32,1,16,128]{4,3,1,2,0:T(8,128)(2,1)}), bf16[16,32,1,16,128]{4,3,1,2,0:T(8,128)(2,1)S(1)}, u32[]{:S(2)}, u32[]{:S(2)}) async-start(bf16[16,32,1,16,128]{4,3,1,2,0:T(8,128)(2,1)} %bitcast.245), calls=%async_computation.1 | async-start | bytes 4194304 | tf_op jit(solution)/shard_map/all_to_all | solution.py:34
  116.3 1.6 slice_bitcast_fusion.29
  117.9 1.6 slice_bitcast_fusion.30
  122.2 3.1 %fusion.5 = bf16[1,2048,128]{2,1,0:T(8,128)(2,1)} fusion(bf16[64,16,2048]{2,1,0:T(8,128)(2,1)} %all-gather.2.cloned.1.call-done, bf16[32,1,16,128]{3,2,0,1:T(8,128)(2,1)} %copy-done.7), kind=kOutput, calls=%fused_computation.14 | convolution fusion | flops 268697600 | bytes 4849664 | tf_op jit(solution)/shard_map/secd,secf->edf/dot_general | solution.py:109
  125.4 38.7 %all-to-all-done.1 = bf16[16,32,1,16,128]{4,3,1,2,0:T(8,128)(2,1)S(1)} async-done(((bf16[16,32,1,16,128]{4,3,1,2,0:T(8,128)(2,1)}), bf16[16,32,1,16,128]{4,3,1,2,0:T(8,128)(2,1)S(1)}, u32[]{:S(2)}, u32[]{:S(2)}) %all-to-all-start.1) | async-done | bytes 2097184 | tf_op jit(solution)/shard_map/all_to_all | solution.py:34
  165.1 9.4 %all-to-all-start.2 = ((bf16[32,16,128]{2,1,0:T(8,128)(2,1)}), bf16[32,16,128]{2,1,0:T(8,128)(2,1)S(1)}, u32[]{:S(2)}, u32[]{:S(2)}) async-start(bf16[32,16,128]{2,1,0:T(8,128)(2,1)} %reduce_sum.97), calls=%async_computation.2 | async-start | bytes 262144 | tf_op jit(solution)/shard_map/all_to_all | solution.py:166
  174.5 3.2 %fusion.4 = bf16[1,2048,128]{2,1,0:T(8,128)(2,1)} fusion(bf16[64,16,2048]{2,1,0:T(8,128)(2,1)} %all-gather.2.cloned.1.call-done, bf16[32,1,16,128]{3,2,0,1:T(8,128)(2,1)S(1)} %get-tuple-element.36), kind=kOutput, calls=%fused_computation.13 | convolution fusion | flops 268697600 | bytes 4849664 | tf_op jit(solution)/shard_map/secd,secf->edf/dot_general | solution.py:112
  177.7 6.0 %all-to-all-done.2 = bf16[32,16,128]{2,1,0:T(8,128)(2,1)S(1)} async-done(((bf16[32,16,128]{2,1,0:T(8,128)(2,1)}), bf16[32,16,128]{2,1,0:T(8,128)(2,1)S(1)}, u32[]{:S(2)}, u32[]{:S(2)}) %all-to-all-start.2) | async-done | bytes 131104 | tf_op jit(solution)/shard_map/all_to_all | solution.py:166
  184.9 18.5 %all_gather.7 = bf16[128,2048]{1,0:T(8,128)(2,1)S(1)} all-gather(bf16[128,128]{1,0:T(8,128)(2,1)S(1)} %add_convert_fusion.1), channel_id=1, replica_groups=mesh['sp'=32,'tp'=16] {'tp'}, dimensions={1}, use_global_device_ids=true | all-gather | bytes 557056 | tf_op jit(solution)/shard_map/all_gather | solution.py:169
  204.4 6.0 %all-to-all-start.5 = ((f32[16,1,256]{2,1,0:T(1,128)}), f32[16,1,256]{2,1,0:T(1,128)S(1)}, u32[]{:S(2)}, u32[]{:S(2)}) async-start(f32[16,1,256]{2,1,0:T(1,128)} %broadcast_in_dim.60), calls=%async_computation.5 | async-start | bytes 32768 | tf_op jit(solution)/shard_map/all_to_all | solution.py:40
  213.6 4.2 %all-to-all-done.5 = f32[16,1,256]{2,1,0:T(1,128)S(1)} async-done(((f32[16,1,256]{2,1,0:T(1,128)}), f32[16,1,256]{2,1,0:T(1,128)S(1)}, u32[]{:S(2)}, u32[]{:S(2)}) %all-to-all-start.5) | async-done | bytes 16416 | tf_op jit(solution)/shard_map/all_to_all | solution.py:40
  217.8 3.9 %all-to-all-start.4 = ((f32[32,1,4096]{2,1,0:T(1,128)}), f32[32,1,4096]{2,1,0:T(1,128)S(1)}, u32[]{:S(2)}, u32[]{:S(2)}) async-start(f32[32,1,4096]{2,1,0:T(1,128)} %reshape.267), calls=%async_computation.4 | async-start | bytes 1048576 | tf_op jit(solution)/shard_map/all_to_all | solution.py:57
  223.1 3.0 %fusion.3 = bf16[1,128,2048]{2,1,0:T(8,128)(2,1)} fusion(bf16[64,16,2048]{2,1,0:T(8,128)(2,1)} %all-gather.2.cloned.1.call-done, f32[32,16,128]{2,1,0:T(8,128)} %copy-done.5, f32[32,16,128]{2,1,0:T(8,128)S(1)} %fusion.12), kind=kOutput, calls=%fused_computation.12 | convolution fusion | flops 269352960 | bytes 3145728 | tf_op jit(solution)/shard_map/secf,secd->efd/dot_general | solution.py:106
  229.4 8.9 %all-to-all-done.4 = f32[32,1,4096]{2,1,0:T(1,128)S(1)} async-done(((f32[32,1,4096]{2,1,0:T(1,128)}), f32[32,1,4096]{2,1,0:T(1,128)S(1)}, u32[]{:S(2)}, u32[]{:S(2)}) %all-to-all-start.4) | async-done | bytes 524320 | tf_op jit(solution)/shard_map/all_to_all | solution.py:57
  238.8 1.9 reduce.6
  (162 shorter events, 28.7 us)
Async XLA Ops:
  7.2 96.1 %copy-start = (bf16[1,2048,128]{2,1,0:T(8,128)(2,1)S(1)}, bf16[1,2048,128]{2,1,0:T(8,128)(2,1)}, u32[]{:S(2)}) copy-start(bf16[1,2048,128]{2,1,0:T(8,128)(2,1)} %param.17) | copy-start | bytes 1572868
  7.2 93.6 %all-gather.2.cloned.1.call-start = ((), (), s32[]{:S(2)}) async-start(), calls=%async_computation.6 | async-start | bytes 4456448 | tf_op jit(solution)/shard_map/all_gather | solution.py:24
  19.6 31.2 %copy-start.6 = (bf16[64,128]{1,0:T(8,128)(2,1)S(1)}, bf16[64,128]{1,0:T(8,128)(2,1)}, u32[]{:S(2)}) copy-start(bf16[64,128]{1,0:T(8,128)(2,1)} %param.24) | copy-start | bytes 49156
  19.6 81.2 %copy-start.4 = (bf16[1,2048,128]{2,1,0:T(8,128)(2,1)S(1)}, bf16[1,2048,128]{2,1,0:T(8,128)(2,1)}, u32[]{:S(2)}) copy-start(bf16[1,2048,128]{2,1,0:T(8,128)(2,1)} %param.18) | copy-start | bytes 1572868
  25.1 80.5 %copy-start.48 = (bf16[1,128,2048]{2,1,0:T(8,128)(2,1)S(1)}, bf16[1,128,2048]{2,1,0:T(8,128)(2,1)}, u32[]{:S(2)}) copy-start(bf16[1,128,2048]{2,1,0:T(8,128)(2,1)} %param.19) | copy-start | bytes 1572868
  51.5 58.3 %all-to-all-start.3 = ((f32[16,1,256]{2,1,0:T(1,128)}), f32[16,1,256]{2,1,0:T(1,128)S(1)}, u32[]{:S(2)}, u32[]{:S(2)}) async-start(f32[16,1,256]{2,1,0:T(1,128)} %broadcast_in_dim.59), calls=%async_computation.3 | async-start | bytes 32768 | tf_op jit(solution)/shard_map/all_to_all | solution.py:40
  110.4 53.7 %all-to-all-start.1 = ((bf16[16,32,1,16,128]{4,3,1,2,0:T(8,128)(2,1)}), bf16[16,32,1,16,128]{4,3,1,2,0:T(8,128)(2,1)S(1)}, u32[]{:S(2)}, u32[]{:S(2)}) async-start(bf16[16,32,1,16,128]{4,3,1,2,0:T(8,128)(2,1)} %bitcast.245), calls=%async_computation.1 | async-start | bytes 4194304 | tf_op jit(solution)/shard_map/all_to_all | solution.py:34
  165.1 18.7 %all-to-all-start.2 = ((bf16[32,16,128]{2,1,0:T(8,128)(2,1)}), bf16[32,16,128]{2,1,0:T(8,128)(2,1)S(1)}, u32[]{:S(2)}, u32[]{:S(2)}) async-start(bf16[32,16,128]{2,1,0:T(8,128)(2,1)} %reduce_sum.97), calls=%async_computation.2 | async-start | bytes 262144 | tf_op jit(solution)/shard_map/all_to_all | solution.py:166
  174.4 29.0 %copy-start.11 = (f32[128]{0:T(128)S(1)}, f32[128]{0:T(128)}, u32[]{:S(2)}) copy-start(f32[128]{0:T(128)} %get-tuple-element.75) | copy-start | bytes 1540
  174.5 29.0 %copy-start.13 = (f32[128]{0:T(128)S(1)}, f32[128]{0:T(128)}, u32[]{:S(2)}) copy-start(f32[128]{0:T(128)} %get-tuple-element.76) | copy-start | bytes 1540
  174.5 29.0 %copy-start.47 = (f32[64]{0:T(128)S(1)}, f32[64]{0:T(128)}, u32[]{:S(2)}) copy-start(f32[64]{0:T(128)} %param.25) | copy-start | bytes 772
  174.5 29.0 %copy-start.49 = (bf16[2048,64]{0,1:T(8,128)(2,1)S(1)}, bf16[2048,64]{0,1:T(8,128)(2,1)}, u32[]{:S(2)}) copy-start(bf16[2048,64]{0,1:T(8,128)(2,1)} %param.20) | copy-start | bytes 786436
  203.4 18.3 %copy-start.12 = (f32[128]{0:T(128)S(1)}, f32[128]{0:T(128)}, u32[]{:S(2)}) copy-start(f32[128]{0:T(128)} %get-tuple-element.75) | copy-start | bytes 1540
  203.4 18.3 %copy-start.14 = (f32[128]{0:T(128)S(1)}, f32[128]{0:T(128)}, u32[]{:S(2)}) copy-start(f32[128]{0:T(128)} %get-tuple-element.76) | copy-start | bytes 1540
  204.4 13.4 %all-to-all-start.5 = ((f32[16,1,256]{2,1,0:T(1,128)}), f32[16,1,256]{2,1,0:T(1,128)S(1)}, u32[]{:S(2)}, u32[]{:S(2)}) async-start(f32[16,1,256]{2,1,0:T(1,128)} %broadcast_in_dim.60), calls=%async_computation.5 | async-start | bytes 32768 | tf_op jit(solution)/shard_map/all_to_all | solution.py:40
  211.2 15.8 %copy-start.8 = (bf16[64,128]{1,0:T(8,128)(2,1)S(1)}, bf16[64,128]{1,0:T(8,128)(2,1)}, u32[]{:S(2)}) copy-start(bf16[64,128]{1,0:T(8,128)(2,1)} %param.22) | copy-start | bytes 49156
  211.2 15.8 %copy-start.10 = (bf16[64,128]{1,0:T(8,128)(2,1)S(1)}, bf16[64,128]{1,0:T(8,128)(2,1)}, u32[]{:S(2)}) copy-start(bf16[64,128]{1,0:T(8,128)(2,1)} %param.21) | copy-start | bytes 49156
  211.2 15.8 %copy-start.16 = (f32[64]{0:T(128)S(1)}, f32[64]{0:T(128)}, u32[]{:S(2)}) copy-start(f32[64]{0:T(128)} %get-tuple-element.59) | copy-start | bytes 772
  211.2 15.8 %copy-start.17 = (f32[64]{0:T(128)S(1)}, f32[64]{0:T(128)}, u32[]{:S(2)}) copy-start(f32[64]{0:T(128)} %get-tuple-element.60) | copy-start | bytes 772
  211.2 15.8 %copy-start.18 = (f32[64]{0:T(128)S(1)}, f32[64]{0:T(128)}, u32[]{:S(2)}) copy-start(f32[64]{0:T(128)} %get-tuple-element.61) | copy-start | bytes 772
  211.2 15.8 %copy-start.19 = (f32[64]{0:T(128)S(1)}, f32[64]{0:T(128)}, u32[]{:S(2)}) copy-start(f32[64]{0:T(128)} %get-tuple-element.62) | copy-start | bytes 772
  211.2 15.8 %copy-start.20 = (f32[64]{0:T(128)S(1)}, f32[64]{0:T(128)}, u32[]{:S(2)}) copy-start(f32[64]{0:T(128)} %get-tuple-element.63) | copy-start | bytes 772
  217.8 20.5 %all-to-all-start.4 = ((f32[32,1,4096]{2,1,0:T(1,128)}), f32[32,1,4096]{2,1,0:T(1,128)S(1)}, u32[]{:S(2)}, u32[]{:S(2)}) async-start(f32[32,1,4096]{2,1,0:T(1,128)} %reshape.267), calls=%async_computation.4 | async-start | bytes 1048576 | tf_op jit(solution)/shard_map/all_to_all | solution.py:57
  221.8 5.2 %collective-permute-start = (f32[64,30]{1,0:T(8,128)S(1)}, f32[64,30]{1,0:T(8,128)S(1)}, u32[]{:S(2)}, u32[]{:S(2)}) collective-permute-start(f32[64,30]{1,0:T(8,128)S(1)} %bitcast.253), channel_id=1, source_target_pairs={{16,0},{32,16},{48,32},{64,48},{80,64},{96,80},{112,96},{128,112},... | collective-permute-start | bytes 23048 | tf_op jit(solution)/shard_map/ppermute | solution.py:64
  (33 other events, 419.2 us)
Sparse Core Ops, SparseCore 0:
  50.9 49.7 all-gather.1
where the time goes:
time: 250 us
  waiting for transfers between devices  98.5 us (39%)
  blocking collectives  43.5 us (17%)
  starting transfers between devices  34.9 us (14%)
  local copies, waits for them, and re-layouts  27.2 us (11%)
  matrix products  16.9 us (7%)
  between operations  15 us (6%)
  other arithmetic  13.7 us (5%)
    all_gather x1, waiting for transfers between devices, sent_together_2(): lax.all_gather(both, axis, axis=dim, tiled=True)  39.7 us
    all_to_all x1, waiting for transfers between devices, summed_on_arrival(): lax.all_to_all(tiles, axis, split_axis=0, concat_axis=0, tiled=True)  38.7 us
    all_to_all x1, blocking collectives, sent_together(): lax.all_to_all(both, axis, split_axis=split_dim, concat_axis=concat_dim,...  24.9 us
    all_gather x1, blocking collectives, body(): grad_stream = lax.all_gather(stream_part, 'tp', axis=1, tiled=True)  18.5 us
    all_to_all x2, starting transfers between devices, copy_for_each(): return lax.all_to_all(copies, axis, split_axis=0, concat_axis=0, tiled=True)  15.6 us
    all_to_all x1, starting transfers between devices, body(): lax.all_to_all(returned, 'sp', split_axis=0, concat_axis=0, tiled=True)  9.38 us
    all_to_all x1, waiting for transfers between devices, summed_on_arrival_2(): lax.all_to_all(cut_along(array, dim, devices), axis, 0, 0, tiled=True)  8.92 us
    all_to_all x1, waiting for transfers between devices, body(): lax.all_to_all(returned, 'sp', split_axis=0, concat_axis=0, tiled=True)  6.04 us
  transfers between devices with their start and end apart: 7, of which 6 were waited for; matrix products, arithmetic and copies ran while one was open for 12% of the time, Pallas kernels for 0%

commit v1 on v0

--- a/solution.py
+++ b/solution.py
@@ -166,7 +166,9 @@
     returned = lax.all_to_all(returned, "sp", split_axis=0, concat_axis=0, tiled=True)
     cot_cols = lax.dynamic_slice_in_dim(out_cot, slice_start, slice_width, 1)
     stream_part = combine_routes(returned, slot_of, cot_cols, token_rows, top_count)
-    grad_stream = lax.all_gather(stream_part, "tp", axis=1, tiled=True)
+    grad_stream = jnp.concatenate(
+        lax.all_to_all(jnp.stack([stream_part] * lax.axis_size("tp")), "tp", 0, 0), axis=1
+    )
     channel_total = conv_result.shape[0] * tp_count
     positions = conv_result.shape[1]
     conv_float = conv_result.astype(jnp.float32)

time: 250 us -> 264 us (1.056)
  waiting for transfers between devices: 98.5 us -> 136 us
  blocking collectives: 43.5 us -> 24.9 us
    all_gather x1 -> x0, blocking collectives: 18.5 us -> none  [body(): grad_stream = lax.all_gather(stream_part, 'tp', axis=1, tiled=True)]
    all_to_all x0 -> x1, waiting for transfers between devices: none -> 12.4 us  [body(): lax.all_to_all(jnp.stack([stream_part] * lax.axis_size('tp')), 'tp', 0, 0)]
    all_gather x1, waiting for transfers between devices: 39.7 us -> 50.3 us  [sent_together_2(): lax.all_gather(both, axis, axis=dim, tiled=True)]
    all_to_all x1, waiting for transfers between devices: 38.7 us -> 46.9 us  [summed_on_arrival(): lax.all_to_all(tiles, axis, split_axis=0, concat_axis=0, tiled=True)]
    all_to_all x2, starting transfers between devices: 15.6 us -> 8.23 us  [copy_for_each(): return lax.all_to_all(copies, axis, split_axis=0, concat_axis=0, tiled=True)]
    all_to_all x0 -> x1, starting transfers between devices: none -> 5.45 us  [body(): lax.all_to_all(jnp.stack([stream_part] * lax.axis_size('tp')), 'tp', 0, 0)]
    all_to_all x2, waiting for transfers between devices: 4.23 us -> 9.65 us  [copy_for_each(): return lax.all_to_all(copies, axis, split_axis=0, concat_axis=0, tiled=True)]
    unnamed x106 -> x99, local copies, waits for them, and re-layouts: 5.75 us -> 4.68 us
  transfers between devices with their start and end apart: 7 -> 8, of which waited for: 6 -> 7; matrix products, arithmetic and copies ran while one was open for 12% -> 7% of each run, Pallas kernels for 0% -> 0%
where the time goes in v1:
time: 264 us; the launch traced here: 263 us
  waiting for transfers between devices  136 us (52%)
  starting transfers between devices  32.4 us (12%)
  local copies, waits for them, and re-layouts  26.8 us (10%)
  blocking collectives  24.9 us (9%)
  matrix products  15.4 us (6%)
  between operations  14.9 us (6%)
  other arithmetic  12.4 us (5%)
    all_gather x1, waiting for transfers between devices, sent_together_2(): lax.all_gather(both, axis, axis=dim, tiled=True)  50.3 us
    all_to_all x1, waiting for transfers between devices, summed_on_arrival(): lax.all_to_all(tiles, axis, split_axis=0, concat_axis=0, tiled=True)  46.9 us
    all_to_all x1, blocking collectives, sent_together(): lax.all_to_all(both, axis, split_axis=split_dim, concat_axis=concat_dim,...  24.9 us
    all_to_all x1, waiting for transfers between devices, body(): lax.all_to_all(jnp.stack([stream_part] * lax.axis_size('tp')), 'tp', 0, 0)  12.4 us
    all_to_all x1, starting transfers between devices, body(): lax.all_to_all(returned, 'sp', split_axis=0, concat_axis=0, tiled=True)  9.69 us
    all_to_all x2, waiting for transfers between devices, copy_for_each(): return lax.all_to_all(copies, axis, split_axis=0, concat_axis=0, tiled=True)  9.65 us
    all_to_all x1, waiting for transfers between devices, summed_on_arrival_2(): lax.all_to_all(cut_along(array, dim, devices), axis, 0, 0, tiled=True)  8.85 us
    all_to_all x2, starting transfers between devices, copy_for_each(): return lax.all_to_all(copies, axis, split_axis=0, concat_axis=0, tiled=True)  8.23 us
  transfers between devices with their start and end apart: 8, of which 7 were waited for; matrix products, arithmetic and copies ran while one was open for 7% of the time, Pallas kernels for 0%

profile of v1, /device:TPU:1, one launch (start us, length us, event | category | flops | bytes accessed | tf_op | source)
XLA Modules:
  0.0 262.7 jit_solution(16035389105693923300)
XLA Ops:
  12.7 3.5 %gather_fusion.1 = f32[512]{0:T(512)S(1)} fusion(f32[256]{0:T(256)S(1)} %reshape.210, s32[1024]{0:T(1024)S(1)} %get-tuple-element.78), kind=kCustom, calls=%fused_computation.1 | custom fusion | bytes 6144 | tf_op jit(solution)/shard_map/gather | solution.py:150
  16.3 3.3 %gather_fusion.2 = bf16[512,2048]{1,0:T(8,128)(2,1)} fusion(bf16[128,2048]{1,0:T(8,128)(2,1)S(1)} %copy-done.1, s32[1024]{0:T(1024)S(1)} %get-tuple-element.79), kind=kCustom, calls=%fused_computation.2 | custom fusion | bytes 4196352 | tf_op jit(solution)/shard_map/gather | solution.py:152
  19.6 3.3 %gather_fusion = bf16[512,2048]{1,0:T(8,128)(2,1)} fusion(bf16[128,2048]{1,0:T(8,128)(2,1)S(1)} %copy-done.2, s32[1024]{0:T(1024)S(1)} %get-tuple-element.79), kind=kCustom, calls=%fused_computation | custom fusion | bytes 4196352 | tf_op jit(solution)/shard_map/gather | solution.py:151
  25.1 24.9 %all_to_all.37 = bf16[32,32,128]{2,1,0:T(8,128)(2,1)S(1)} all-to-all(bf16[32,32,128]{2,1,0:T(8,128)(2,1)S(1)} %pad_maximum_fusion), channel_id=1, replica_groups=mesh['sp'=32,'tp'=16] {'sp'}, dimensions={0} | all-to-all | bytes 524288 | tf_op jit(solution)/shard_map/all_to_all | solution.py:14
  50.8 50.3 %all-gather.2.cloned.1.call-done = bf16[64,16,2048]{2,1,0:T(8,128)(2,1)} async-done(((bf16[64,16,128]{2,1,0:T(8,128)(2,1)}), bf16[64,16,2048]{2,1,0:T(8,128)(2,1)}) %all-gather.2.cloned.1.call-update) | async-done | bytes 4194320 | tf_op jit(solution)/shard_map/all_gather | solution.py:24
  101.1 2.4 fusion.12
  103.6 2.3 fusion.17
  108.2 1.9 copy.82
  110.1 3.8 %all-to-all-start.1 = ((bf16[16,32,1,16,128]{4,3,1,2,0:T(8,128)(2,1)}), bf16[16,32,1,16,128]{4,3,1,2,0:T(8,128)(2,1)S(1)}, u32[]{:S(2)}, u32[]{:S(2)}) async-start(bf16[16,32,1,16,128]{4,3,1,2,0:T(8,128)(2,1)} %bitcast.254), calls=%async_computation.1 | async-start | bytes 4194304 | tf_op jit(solution)/shard_map/all_to_all | solution.py:34
  114.5 1.6 slice_bitcast_fusion.30
  116.1 46.9 %all-to-all-done.1 = bf16[16,32,1,16,128]{4,3,1,2,0:T(8,128)(2,1)S(1)} async-done(((bf16[16,32,1,16,128]{4,3,1,2,0:T(8,128)(2,1)}), bf16[16,32,1,16,128]{4,3,1,2,0:T(8,128)(2,1)S(1)}, u32[]{:S(2)}, u32[]{:S(2)}) %all-to-all-start.1) | async-done | bytes 2097184 | tf_op jit(solution)/shard_map/all_to_all | solution.py:34
  164.3 4.8 %all-to-all-start.4 = ((f32[16,1,256]{2,1,0:T(1,128)}), f32[16,1,256]{2,1,0:T(1,128)}, u32[]{:S(2)}, u32[]{:S(2)}) async-start(f32[16,1,256]{2,1,0:T(1,128)} %broadcast_in_dim.59), calls=%async_computation.4 | async-start | bytes 32768 | tf_op jit(solution)/shard_map/all_to_all | solution.py:40
  171.7 4.9 %all-to-all-done.4 = f32[16,1,256]{2,1,0:T(1,128)} async-done(((f32[16,1,256]{2,1,0:T(1,128)}), f32[16,1,256]{2,1,0:T(1,128)}, u32[]{:S(2)}, u32[]{:S(2)}) %all-to-all-start.4) | async-done | bytes 16416 | tf_op jit(solution)/shard_map/all_to_all | solution.py:40
  176.6 9.7 %all-to-all-start.2 = ((bf16[32,16,128]{2,1,0:T(8,128)(2,1)}), bf16[32,16,128]{2,1,0:T(8,128)(2,1)S(1)}, u32[]{:S(2)}, u32[]{:S(2)}) async-start(bf16[32,16,128]{2,1,0:T(8,128)(2,1)} %reduce_sum.97), calls=%async_computation.2 | async-start | bytes 262144 | tf_op jit(solution)/shard_map/all_to_all | solution.py:166
  187.7 7.9 %all-to-all-done.2 = bf16[32,16,128]{2,1,0:T(8,128)(2,1)S(1)} async-done(((bf16[32,16,128]{2,1,0:T(8,128)(2,1)}), bf16[32,16,128]{2,1,0:T(8,128)(2,1)S(1)}, u32[]{:S(2)}, u32[]{:S(2)}) %all-to-all-start.2) | async-done | bytes 131104 | tf_op jit(solution)/shard_map/all_to_all | solution.py:166
  197.6 5.5 %all-to-all-start.3 = ((bf16[16,128,128]{2,1,0:T(8,128)(2,1)}), bf16[16,128,128]{2,1,0:T(8,128)(2,1)S(1)}, u32[]{:S(2)}, u32[]{:S(2)}) async-start(bf16[16,128,128]{2,1,0:T(8,128)(2,1)} %stack.2), calls=%async_computation.3 | async-start | bytes 1048576 | tf_op jit(solution)/shard_map/all_to_all | solution.py:170
  203.0 3.3 %fusion.5 = bf16[1,2048,128]{2,1,0:T(8,128)(2,1)} fusion(bf16[64,16,2048]{2,1,0:T(8,128)(2,1)} %all-gather.2.cloned.1.call-done, bf16[32,1,16,128]{3,2,0,1:T(8,128)(2,1)} %copy-done.10), kind=kOutput, calls=%fused_computation.14 | convolution fusion | flops 268697600 | bytes 4849664 | tf_op jit(solution)/shard_map/secd,secf->edf/dot_general | solution.py:109
  207.9 12.4 %all-to-all-done.3 = bf16[16,128,128]{2,1,0:T(8,128)(2,1)S(1)} async-done(((bf16[16,128,128]{2,1,0:T(8,128)(2,1)}), bf16[16,128,128]{2,1,0:T(8,128)(2,1)S(1)}, u32[]{:S(2)}, u32[]{:S(2)}) %all-to-all-start.3) | async-done | bytes 524320 | tf_op jit(solution)/shard_map/all_to_all | solution.py:170
  221.4 3.4 %all-to-all-start.6 = ((f32[16,1,256]{2,1,0:T(1,128)}), f32[16,1,256]{2,1,0:T(1,128)S(1)}, u32[]{:S(2)}, u32[]{:S(2)}) async-start(f32[16,1,256]{2,1,0:T(1,128)} %broadcast_in_dim.60), calls=%async_computation.6 | async-start | bytes 32768 | tf_op jit(solution)/shard_map/all_to_all | solution.py:40
  227.0 4.8 %all-to-all-done.6 = f32[16,1,256]{2,1,0:T(1,128)S(1)} async-done(((f32[16,1,256]{2,1,0:T(1,128)}), f32[16,1,256]{2,1,0:T(1,128)S(1)}, u32[]{:S(2)}, u32[]{:S(2)}) %all-to-all-start.6) | async-done | bytes 16416 | tf_op jit(solution)/shard_map/all_to_all | solution.py:40
  231.8 3.9 %all-to-all-start.5 = ((f32[32,1,4096]{2,1,0:T(1,128)}), f32[32,1,4096]{2,1,0:T(1,128)S(1)}, u32[]{:S(2)}, u32[]{:S(2)}) async-start(f32[32,1,4096]{2,1,0:T(1,128)} %reshape.276), calls=%async_computation.5 | async-start | bytes 1048576 | tf_op jit(solution)/shard_map/all_to_all | solution.py:57
  237.1 2.9 %fusion.3 = bf16[1,128,2048]{2,1,0:T(8,128)(2,1)} fusion(bf16[64,16,2048]{2,1,0:T(8,128)(2,1)} %all-gather.2.cloned.1.call-done, f32[32,16,128]{2,1,0:T(8,128)S(1)} %copy-done.9, f32[32,16,128]{2,1,0:T(8,128)S(1)} %fusion.12), kind=kOutput, calls=%fused_computation.12 | convolution fusion | flops 269352960 | bytes 3145728 | tf_op jit(solution)/shard_map/secf,secd->efd/dot_general | solution.py:106
  243.5 8.9 %all-to-all-done.5 = f32[32,1,4096]{2,1,0:T(1,128)S(1)} async-done(((f32[32,1,4096]{2,1,0:T(1,128)}), f32[32,1,4096]{2,1,0:T(1,128)S(1)}, u32[]{:S(2)}, u32[]{:S(2)}) %all-to-all-start.5) | async-done | bytes 524320 | tf_op jit(solution)/shard_map/all_to_all | solution.py:57
  252.8 1.9 reduce.6
  (156 shorter events, 29.4 us)
Async XLA Ops:
  7.2 96.4 %copy-start = (bf16[1,2048,128]{2,1,0:T(8,128)(2,1)S(1)}, bf16[1,2048,128]{2,1,0:T(8,128)(2,1)}, u32[]{:S(2)}) copy-start(bf16[1,2048,128]{2,1,0:T(8,128)(2,1)} %param.17) | copy-start | bytes 1572868
  7.2 93.9 %all-gather.2.cloned.1.call-start = ((), (), s32[]{:S(2)}) async-start(), calls=%async_computation.7 | async-start | bytes 4456448 | tf_op jit(solution)/shard_map/all_gather | solution.py:24
  19.6 81.5 %copy-start.5 = (bf16[1,2048,128]{2,1,0:T(8,128)(2,1)S(1)}, bf16[1,2048,128]{2,1,0:T(8,128)(2,1)}, u32[]{:S(2)}) copy-start(bf16[1,2048,128]{2,1,0:T(8,128)(2,1)} %param.18) | copy-start | bytes 1572868
  25.0 80.8 %copy-start.46 = (bf16[1,128,2048]{2,1,0:T(8,128)(2,1)S(1)}, bf16[1,128,2048]{2,1,0:T(8,128)(2,1)}, u32[]{:S(2)}) copy-start(bf16[1,128,2048]{2,1,0:T(8,128)(2,1)} %param.19) | copy-start | bytes 1572868
  110.1 52.9 %all-to-all-start.1 = ((bf16[16,32,1,16,128]{4,3,1,2,0:T(8,128)(2,1)}), bf16[16,32,1,16,128]{4,3,1,2,0:T(8,128)(2,1)S(1)}, u32[]{:S(2)}, u32[]{:S(2)}) async-start(bf16[16,32,1,16,128]{4,3,1,2,0:T(8,128)(2,1)} %bitcast.254), calls=%async_computation.1 | async-start | bytes 4194304 | tf_op jit(solution)/shard_map/all_to_all | solution.py:34
  164.3 12.3 %all-to-all-start.4 = ((f32[16,1,256]{2,1,0:T(1,128)}), f32[16,1,256]{2,1,0:T(1,128)}, u32[]{:S(2)}, u32[]{:S(2)}) async-start(f32[16,1,256]{2,1,0:T(1,128)} %broadcast_in_dim.59), calls=%async_computation.4 | async-start | bytes 32768 | tf_op jit(solution)/shard_map/all_to_all | solution.py:40
  176.6 19.0 %all-to-all-start.2 = ((bf16[32,16,128]{2,1,0:T(8,128)(2,1)}), bf16[32,16,128]{2,1,0:T(8,128)(2,1)S(1)}, u32[]{:S(2)}, u32[]{:S(2)}) async-start(bf16[32,16,128]{2,1,0:T(8,128)(2,1)} %reduce_sum.97), calls=%async_computation.2 | async-start | bytes 262144 | tf_op jit(solution)/shard_map/all_to_all | solution.py:166
  197.6 22.7 %all-to-all-start.3 = ((bf16[16,128,128]{2,1,0:T(8,128)(2,1)}), bf16[16,128,128]{2,1,0:T(8,128)(2,1)S(1)}, u32[]{:S(2)}, u32[]{:S(2)}) async-start(bf16[16,128,128]{2,1,0:T(8,128)(2,1)} %stack.2), calls=%async_computation.3 | async-start | bytes 1048576 | tf_op jit(solution)/shard_map/all_to_all | solution.py:170
  207.9 29.1 %copy-start.9 = (f32[32,16,128]{2,1,0:T(8,128)S(1)}, f32[32,16,128]{2,1,0:T(8,128)}, u32[]{:S(2)}) copy-start(f32[32,16,128]{2,1,0:T(8,128)} %copy-done.8) | copy-start | bytes 786436
  221.4 10.3 %all-to-all-start.6 = ((f32[16,1,256]{2,1,0:T(1,128)}), f32[16,1,256]{2,1,0:T(1,128)S(1)}, u32[]{:S(2)}, u32[]{:S(2)}) async-start(f32[16,1,256]{2,1,0:T(1,128)} %broadcast_in_dim.60), calls=%async_computation.6 | async-start | bytes 32768 | tf_op jit(solution)/shard_map/all_to_all | solution.py:40
  224.8 16.2 %copy-start.11 = (bf16[64,128]{1,0:T(8,128)(2,1)S(1)}, bf16[64,128]{1,0:T(8,128)(2,1)}, u32[]{:S(2)}) copy-start(bf16[64,128]{1,0:T(8,128)(2,1)} %param.22) | copy-start | bytes 49156
  224.9 16.1 %copy-start.12 = (bf16[64,128]{1,0:T(8,128)(2,1)S(1)}, bf16[64,128]{1,0:T(8,128)(2,1)}, u32[]{:S(2)}) copy-start(bf16[64,128]{1,0:T(8,128)(2,1)} %param.21) | copy-start | bytes 49156
  224.9 16.1 %copy-start.15 = (f32[64]{0:T(128)S(1)}, f32[64]{0:T(128)}, u32[]{:S(2)}) copy-start(f32[64]{0:T(128)} %get-tuple-element.40) | copy-start | bytes 772
  224.9 16.1 %copy-start.16 = (f32[64]{0:T(128)S(1)}, f32[64]{0:T(128)}, u32[]{:S(2)}) copy-start(f32[64]{0:T(128)} %get-tuple-element.41) | copy-start | bytes 772
  224.9 16.1 %copy-start.17 = (f32[64]{0:T(128)S(1)}, f32[64]{0:T(128)}, u32[]{:S(2)}) copy-start(f32[64]{0:T(128)} %get-tuple-element.42) | copy-start | bytes 772
  224.9 16.1 %copy-start.18 = (f32[64]{0:T(128)S(1)}, f32[64]{0:T(128)}, u32[]{:S(2)}) copy-start(f32[64]{0:T(128)} %get-tuple-element.43) | copy-start | bytes 772
  224.9 16.1 %copy-start.19 = (f32[64]{0:T(128)S(1)}, f32[64]{0:T(128)}, u32[]{:S(2)}) copy-start(f32[64]{0:T(128)} %get-tuple-element.44) | copy-start | bytes 772
  224.9 16.1 %copy-start.20 = (f32[64]{0:T(128)S(1)}, f32[64]{0:T(128)}, u32[]{:S(2)}) copy-start(f32[64]{0:T(128)} %get-tuple-element.45) | copy-start | bytes 772
  224.9 16.1 %copy-start.21 = (f32[64]{0:T(128)S(1)}, f32[64]{0:T(128)}, u32[]{:S(2)}) copy-start(f32[64]{0:T(128)} %get-tuple-element.46) | copy-start | bytes 772
  224.9 16.1 %copy-start.22 = (f32[64]{0:T(128)S(1)}, f32[64]{0:T(128)}, u32[]{:S(2)}) copy-start(f32[64]{0:T(128)} %get-tuple-element.47) | copy-start | bytes 772
  225.0 16.1 %copy-start.23 = (f32[64]{0:T(128)S(1)}, f32[64]{0:T(128)}, u32[]{:S(2)}) copy-start(f32[64]{0:T(128)} %get-tuple-element.48) | copy-start | bytes 772
  225.0 16.1 %copy-start.24 = (f32[64]{0:T(128)S(1)}, f32[64]{0:T(128)}, u32[]{:S(2)}) copy-start(f32[64]{0:T(128)} %get-tuple-element.49) | copy-start | bytes 772
  231.8 20.5 %all-to-all-start.5 = ((f32[32,1,4096]{2,1,0:T(1,128)}), f32[32,1,4096]{2,1,0:T(1,128)S(1)}, u32[]{:S(2)}, u32[]{:S(2)}) async-start(f32[32,1,4096]{2,1,0:T(1,128)} %reshape.276), calls=%async_computation.5 | async-start | bytes 1048576 | tf_op jit(solution)/shard_map/all_to_all | solution.py:57
  235.7 5.3 %collective-permute-start = (f32[64,30]{1,0:T(8,128)S(1)}, f32[64,30]{1,0:T(8,128)S(1)}, u32[]{:S(2)}, u32[]{:S(2)}) collective-permute-start(f32[64,30]{1,0:T(8,128)S(1)} %bitcast.259), channel_id=1, source_target_pairs={{16,0},{32,16},{48,32},{64,48},{80,64},{96,80},{112,96},{128,112},... | collective-permute-start | bytes 23048 | tf_op jit(solution)/shard_map/ppermute | solution.py:64
  (31 other events, 398.0 us)
Sparse Core Ops, SparseCore 0:
  50.9 50.1 all-gather.1
